TPU v7x, 512 devices: a whole 4x4x16 slice. The times are simulated.
512 devices in a mesh: sp: 64 (over z, y), dp: 8 (over x, core).
Axes of the slice: x: 4, y: 4, z: 16, core: 2. Of those that a mesh axis runs over, the one named last changes fastest.
Arguments:
- gate_input: bfloat16 [8, 12288, 4096], P('dp', 'sp'), may hold values from -6 to 6
- value_input: bfloat16 [8, 12288, 4096], P('dp', 'sp'), may hold values from -6 to 6
- norm_gain: float32 [4096], replicated, may hold values from 0.1 to 1.9
- norm_bias: float32 [4096], replicated, may hold values from -3 to 3
- mix_weight: bfloat16 [64, 1024, 1024], P('sp', 'dp'), may hold values from -0.1875 to 0.1875
- mix_bias: float32 [64, 1024], P('sp'), may hold values from 0.1 to 1.9
Outputs:
- gated: bfloat16 [8, 12288, 4096], P('dp', 'sp')
All inputs are finite; a program needn't handle non-finite values.
Results may differ from a plain program's by a relative error of at most 0.0053.
Values may be sent and summed in bfloat16 or wider, within the bound.
No kernel may reach another device: no remote copies, remote signals or barrier semaphores. Data moves between devices by JAX's collectives and lax.ppermute only.
A program may use at most 64 MiB of HBM per device.

v0:
```python
import jax
import jax.numpy as jnp
from jax import lax
from jax.sharding import Mesh
from jax.sharding import PartitionSpec as P

GROUP_DIM = 64
SPAN = 1024
DP = ("dp_0", "dp_1")
epsilon = 1e-05


def joined_along(parts, dim):
    parts = jnp.moveaxis(parts, 0, dim)
    lengths = parts.shape
    return parts.reshape(*lengths[:dim], lengths[dim] * lengths[dim + 1], *lengths[dim + 2 :])


def all_blocks(shard, axes, sequence):
    parts = shard[None]
    for k in sequence:
        parts = lax.all_gather(parts, axes[k], axis=0, tiled=True)
    current = [lax.axis_size(axes[k]) for k in reversed(sequence)]
    parts = parts.reshape(*current, *shard.shape)
    turned = sorted(range(len(sequence)), key=lambda place: sequence[len(sequence) - 1 - place])
    return parts.transpose(*turned, *range(len(sequence), parts.ndim)).reshape(-1, *shard.shape)


def gather_axes(shard, axes, sequence, dim):
    return joined_along(all_blocks(shard, axes, sequence), dim)


def local(gate_input, value_input, norm_gain, norm_bias, mix_weight, mix_bias):
    token_rows = value_input.shape[1]
    channels = value_input.shape[2]
    act_value = jax.nn.gelu(value_input[0].astype(jnp.float32))
    centre = jnp.mean(act_value, axis=-1, keepdims=True)
    shifted = act_value - centre
    variance = jnp.mean(shifted * shifted, axis=-1, keepdims=True)
    normed = (shifted * lax.rsqrt(variance + epsilon) * norm_gain + norm_bias).astype(jnp.bfloat16)
    normed_group = lax.all_to_all(normed, "sp", split_axis=1, concat_axis=0, tiled=True)
    positions = normed_group.shape[0]
    group_count = mix_weight.shape[0]
    blocks = normed_group.reshape(positions // SPAN, SPAN, group_count, GROUP_DIM)
    columns = lax.broadcasted_iota(jnp.int32, (1, SPAN), 1)
    weight_rows = gather_axes(mix_weight, DP, (0, 1), 1)
    row_count = weight_rows.shape[1]
    rows_index = lax.broadcasted_iota(jnp.int32, (row_count, 1), 0)
    masked = jnp.where((columns <= rows_index)[None], weight_rows, jnp.zeros_like(weight_rows))
    summed = jnp.einsum("gqp,npgc->nqgc", masked, blocks, preferred_element_type=jnp.float32)
    mixed_blocks = (summed + mix_bias.T[None, :, :, None]).astype(jnp.bfloat16)
    mixed_flat = lax.optimization_barrier(mixed_blocks.reshape(positions, group_count * GROUP_DIM))
    returned = lax.all_to_all(mixed_flat, "sp", split_axis=0, concat_axis=1, tiled=True)
    gated_rows = (
        jax.nn.gelu(gate_input[0].astype(jnp.float32)) * returned.astype(jnp.float32)
    ).astype(jnp.bfloat16)
    return gated_rows.reshape(1, token_rows, channels)


def solution(mesh):
    split = Mesh(mesh.devices.reshape(mesh.shape["sp"], 4, 2), ("sp", "dp_0", "dp_1"))
    in_specs = (P(DP, "sp", None), P(DP, "sp", None), P(), P(), P("sp", DP, None), P("sp", None))
    out_specs = P(DP, "sp", None)
    return jax.shard_map(local, mesh=split, in_specs=in_specs, out_specs=out_specs, check_vma=False)
```

profile of v0, /device:TPU:2, one launch (start us, length us, event | category | flops | bytes accessed | tf_op | source)
XLA Modules:
  0.0 276.7 jit_solution(663343438426462109)
XLA Ops:
  6.5 0.8 mul.82
  7.3 0.8 add.70
  8.1 3.1 %copy.24 = bf16[1,192,4096]{1,2,0:T(8,128)(2,1)S(1)} copy(bf16[1,192,4096]{2,1,0:T(8,128)(2,1)} %param.7) | data formatting | bytes 3145728 | tf_op args[1]
  11.3 1.6 fusion.28
  12.8 1.8 multiply_reduce_fusion
  14.7 3.1 %fusion.18 = bf16[192,64,64]{0,2,1:T(8,128)(2,1)} fusion(f32[64,64]{1,0:T(8,128)S(1)} %add.70, f32[64,64]{1,0:T(8,128)S(1)} %mul.82, f32[192]{0:T(256)S(1)} %add_rsqrt_fusion, f32[192]{0:T(256)S(1)} %broadcast_multiply_fusion, bf16[192,64,64]{0,2,1:T(8,128)(2,1)S(1)} %bitcast.43), kind=kLoop, calls=%fused_computation.26 | loop fusion | flops 11010048 | bytes 3180032 | tf_op jit(solution)/shard_map/convert_element_type | solution.py:40
  17.8 18.7 %all-to-all-start = ((bf16[192,64,64]{0,2,1:T(8,128)(2,1)}), bf16[192,64,64]{0,2,1:T(8,128)(2,1)S(1)}, u32[]{:S(2)}, u32[]{:S(2)}) async-start(bf16[192,64,64]{0,2,1:T(8,128)(2,1)} %fusion.18), calls=%async_computation | async-start | bytes 4194304 | tf_op jit(solution)/shard_map/all_to_all | solution.py:41
  36.6 0.0 all-gather.5.cloned.1.call-start
  36.6 0.7 all-gather.5.cloned.1.call-update
  37.3 0.2 all-gather.7.cloned.1.call-start
  37.5 33.0 %all-gather.5.cloned.1.call-done = bf16[4,128,1024]{2,1,0:T(8,128)(2,1)} async-done(((bf16[1,128,1024]{2,1,0:T(8,128)(2,1)}), bf16[4,128,1024]{2,1,0:T(8,128)(2,1)}) %all-gather.5.cloned.1.call-update) | async-done | bytes 1048592 | tf_op jit(solution)/shard_map/all_gather | solution.py:22
  70.6 0.0 all-gather.7.cloned.1.call-update
  70.6 25.0 %all-gather.7.cloned.1.call-done = bf16[8,128,1024]{2,1,0:T(8,128)(2,1)} async-done(((bf16[4,128,1024]{2,1,0:T(8,128)(2,1)}), bf16[8,128,1024]{2,1,0:T(8,128)(2,1)}) %all-gather.7.cloned.1.call-update) | async-done | bytes 2097168 | tf_op jit(solution)/shard_map/all_gather | solution.py:22
  95.7 2.2 fusion.19
  97.9 1.5 copy.26
  99.5 37.3 %all-to-all-done = bf16[192,64,64]{0,2,1:T(8,128)(2,1)S(1)} async-done(((bf16[192,64,64]{0,2,1:T(8,128)(2,1)}), bf16[192,64,64]{0,2,1:T(8,128)(2,1)S(1)}, u32[]{:S(2)}, u32[]{:S(2)}) %all-to-all-start) | async-done | bytes 1572896 | tf_op jit(solution)/shard_map/all_to_all | solution.py:41
  136.8 0.0 copy-start.1
  136.8 2.5 copy.25
  139.3 0.0 copy-start
  139.3 5.4 %reshape.112 = bf16[12,1024,64]{1,0,2:T(8,128)(2,1)} reshape(bf16[64,192,64]{1,0,2:T(8,128)(2,1)} %copy.25) | data formatting | bytes 3145728 | tf_op jit(solution)/shard_map/reshape.1
  144.8 0.0 copy-done.1
  144.8 0.0 copy-done
  144.8 3.8 %fusion.33 = bf16[8,8,12,1024]{3,1,0,2:T(8,128)(2,1)S(1)} fusion(f32[1024]{0:T(1024)S(1)} %bitcast.49, bf16[1024,1024,1]{1,0,2:T(8,128)(2,1)S(1)} %bitcast.48, bf16[12,1024,64]{1,0,2:T(8,128)(2,1)} %reshape.112), kind=kOutput, calls=%fused_computation.43 | convolution fusion | flops 1612185600 | bytes 5246976 | tf_op jit(solution)/shard_map/gqp,npgc->nqgc/dot_general | solution.py:50
  148.5 1.3 copy.31
  149.8 3.6 %all_to_all.22 = bf16[64,192,64]{1,0,2:T(8,128)(2,1)S(1)} reshape(bf16[12288,64]{0,1:T(8,128)(2,1)} %bitcast.46) | data formatting | bytes 3145728 | tf_op jit(solution)/shard_map/all_to_all | solution.py:53
  153.4 1.2 copy.29
  154.6 105.4 %all_to_all.26 = bf16[64,192,64]{1,2,0:T(8,128)(2,1)S(1)} all-to-all(bf16[64,192,64]{1,2,0:T(8,128)(2,1)S(1)} %copy.29), channel_id=1, replica_groups=mesh['sp'=64,'dp_0'=4,'dp_1'=2] {'sp'}, dimensions={0} | all-to-all | bytes 3145728 | tf_op jit(solution)/shard_map/all_to_all | solution.py:53
  259.9 2.5 convert_element_type.61
  262.4 3.7 %copy.30 = f32[1,192,4096]{2,1,0:T(8,128)S(1)} copy(f32[1,192,4096]{1,2,0:T(8,128)} %bitcast.44) | data formatting | bytes 6291456 | tf_op jit(solution)/shard_map/convert_element_type | solution.py:55
  266.2 3.7 %fusion.26 = bf16[1,192,4096]{2,1,0:T(8,128)(2,1)} fusion(f32[1,192,4096]{2,1,0:T(8,128)S(1)} %copy.30, bf16[1,192,4096]{2,1,0:T(8,128)(2,1)} %param.6), kind=kLoop, calls=%fused_computation.34 | loop fusion | flops 8650752 | bytes 6291456 | tf_op jit(solution)/shard_map/convert_element_type | solution.py:56
  (3 shorter events, 0.0 us)
Async XLA Ops:
  17.8 119.0 %all-to-all-start = ((bf16[192,64,64]{0,2,1:T(8,128)(2,1)}), bf16[192,64,64]{0,2,1:T(8,128)(2,1)S(1)}, u32[]{:S(2)}, u32[]{:S(2)}) async-start(bf16[192,64,64]{0,2,1:T(8,128)(2,1)} %fusion.18), calls=%async_computation | async-start | bytes 4194304 | tf_op jit(solution)/shard_map/all_to_all | solution.py:41
  36.6 34.0 %all-gather.5.cloned.1.call-start = ((), (), s32[]{:S(2)}) async-start(), calls=%async_computation.2 | async-start | bytes 1310720 | tf_op jit(solution)/shard_map/all_gather | solution.py:22
  37.3 58.4 %all-gather.7.cloned.1.call-start = ((), (), s32[]{:S(2)}) async-start(), calls=%async_computation.3 | async-start | bytes 3145728 | tf_op jit(solution)/shard_map/all_gather | solution.py:22
  136.8 7.9 %copy-start.1 = (f32[1,1024]{1,0:T(1,128)S(1)}, f32[1,1024]{1,0:T(1,128)}, u32[]{:S(2)}) copy-start(f32[1,1024]{1,0:T(1,128)} %param.11) | copy-start | bytes 12292
  139.3 5.4 %copy-start = (bf16[4,2,1,128,1024]{4,3,1,0,2:T(8,128)(2,1)S(1)}, bf16[4,2,1,128,1024]{4,3,1,0,2:T(8,128)(2,1)}, u32[]{:S(2)}) copy-start(bf16[4,2,1,128,1024]{4,3,1,0,2:T(8,128)(2,1)} %copy.26) | copy-start | bytes 6291460
Sparse Core Ops, SparseCore 0:
  39.5 31.0 all-gather.4
  72.7 22.9 all-gather.6
where the time goes:
time: 277 us
  blocking collectives  105 us (38%)
  waiting for transfers between devices  96.1 us (35%)
  local copies, waits for them, and re-layouts  24 us (9%)
  starting transfers between devices  19 us (7%)
  other arithmetic  15.1 us (5%)
  between operations  13.5 us (5%)
  matrix products  3.76 us (1%)
    all_to_all x1, blocking collectives, local(): lax.all_to_all(mixed_flat, 'sp', split_axis=0, concat_axis=1, tiled=True)  105 us
    all_gather x2, waiting for transfers between devices, all_blocks(): parts = lax.all_gather(parts, axes[k], axis=0, tiled=True)  58.1 us
    all_to_all x1, waiting for transfers between devices, local(): lax.all_to_all(normed, 'sp', split_axis=1, concat_axis=0, tiled=True)  37.3 us
    all_to_all x1, starting transfers between devices, local(): lax.all_to_all(normed, 'sp', split_axis=1, concat_axis=0, tiled=True)  18.7 us
  transfers between devices with their start and end apart: 3, of which 3 were waited for; matrix products, arithmetic and copies ran while one was open for 1% of the time, Pallas kernels for 0%

commit v1 on v0

--- a/solution.py
+++ b/solution.py
@@ -19,7 +19,9 @@
 def all_blocks(shard, axes, sequence):
     parts = shard[None]
     for k in sequence:
-        parts = lax.all_gather(parts, axes[k], axis=0, tiled=True)
+        parts = jnp.concatenate(
+            lax.all_to_all(jnp.stack([parts] * lax.axis_size(axes[k])), axes[k], 0, 0), axis=0
+        )
     current = [lax.axis_size(axes[k]) for k in reversed(sequence)]
     parts = parts.reshape(*current, *shard.shape)
     turned = sorted(range(len(sequence)), key=lambda place: sequence[len(sequence) - 1 - place])

time: 277 us -> 279 us (level)
  the two profiles are of different devices: /device:TPU:2 before, /device:TPU:8 now
where the time goes in v1:
time: 279 us
  blocking collectives  111 us (40%)
  waiting for transfers between devices  103 us (37%)
  starting transfers between devices  23.2 us (8%)
  local copies, waits for them, and re-layouts  21.7 us (8%)
  other arithmetic  15 us (5%)
  matrix products  4.37 us (2%)
    all_to_all x1, blocking collectives, local(): lax.all_to_all(mixed_flat, 'sp', split_axis=0, concat_axis=1, tiled=True)  105 us
    all_to_all x1, waiting for transfers between devices, local(): lax.all_to_all(normed, 'sp', split_axis=1, concat_axis=0, tiled=True)  98.3 us
    all_to_all x1, starting transfers between devices, local(): lax.all_to_all(normed, 'sp', split_axis=1, concat_axis=0, tiled=True)  18.9 us
  transfers between devices with their start and end apart: 2, of which 2 were waited for; matrix products, arithmetic and copies ran while one was open for 4% of the time, Pallas kernels for 0%

profile of v1, /device:TPU:8, one launch (start us, length us, event | category | flops | bytes accessed | tf_op | source)
XLA Modules:
  0.0 278.6 jit_solution(8794174387962564018)
XLA Ops:
  0.0 0.0 copy-start
  0.0 0.0 copy-start.1
  0.0 2.1 stack.6
  2.1 4.3 %all-to-all-start.1 = ((bf16[4,1,1,128,1024]{4,3,2,1,0:T(8,128)(2,1)}), bf16[4,1,1,128,1024]{4,3,2,1,0:T(8,128)(2,1)S(1)}, u32[]{:S(2)}, u32[]{:S(2)}) async-start(bf16[4,1,1,128,1024]{4,3,2,1,0:T(8,128)(2,1)} %stack.6), calls=%async_computation.1 | async-start | bytes 2097152 | tf_op jit(solution)/shard_map/all_to_all | solution.py:23
  6.4 0.0 copy-done
  6.4 0.1 mul.82
  6.4 0.0 copy-done.1
  6.4 0.1 add.70
  6.5 3.1 %copy.29 = bf16[1,192,4096]{1,2,0:T(8,128)(2,1)S(1)} copy(bf16[1,192,4096]{2,1,0:T(8,128)(2,1)} %param.7) | data formatting | bytes 3145728 | tf_op args[1]
  9.7 1.6 fusion.28
  11.3 1.8 multiply_reduce_fusion
  13.1 3.2 %fusion.18 = bf16[192,64,64]{0,2,1:T(8,128)(2,1)} fusion(f32[64,64]{1,0:T(8,128)S(1)} %add.70, f32[64,64]{1,0:T(8,128)S(1)} %mul.82, f32[192]{0:T(256)S(1)} %add_rsqrt_fusion, f32[192]{0:T(256)S(1)} %broadcast_multiply_fusion, bf16[192,64,64]{0,2,1:T(8,128)(2,1)S(1)} %bitcast.44), kind=kLoop, calls=%fused_computation.26 | loop fusion | flops 11010048 | bytes 3180032 | tf_op jit(solution)/shard_map/convert_element_type | solution.py:42
  16.3 5.2 %all-to-all-done.1 = bf16[4,1,1,128,1024]{4,3,2,1,0:T(8,128)(2,1)S(1)} async-done(((bf16[4,1,1,128,1024]{4,3,2,1,0:T(8,128)(2,1)}), bf16[4,1,1,128,1024]{4,3,2,1,0:T(8,128)(2,1)S(1)}, u32[]{:S(2)}, u32[]{:S(2)}) %all-to-all-start.1) | async-done | bytes 1048608 | tf_op jit(solution)/shard_map/all_to_all | solution.py:23
  21.5 0.2 pad_maximum_fusion
  21.6 5.4 %all_to_all.36 = bf16[2,4,1,128,1024]{4,3,1,2,0:T(8,128)(2,1)S(1)} all-to-all(bf16[2,4,1,128,1024]{4,3,1,2,0:T(8,128)(2,1)S(1)} %pad_maximum_fusion), channel_id=1, replica_groups=mesh['sp'=64,'dp_0'=4,'dp_1'=2] {'dp_1'}, dimensions={0} | all-to-all | bytes 4194304 | tf_op jit(solution)/shard_map/all_to_all | solution.py:23
  27.1 18.9 %all-to-all-start = ((bf16[192,64,64]{0,2,1:T(8,128)(2,1)}), bf16[192,64,64]{0,2,1:T(8,128)(2,1)}, u32[]{:S(2)}, u32[]{:S(2)}) async-start(bf16[192,64,64]{0,2,1:T(8,128)(2,1)} %fusion.18), calls=%async_computation | async-start | bytes 4194304 | tf_op jit(solution)/shard_map/all_to_all | solution.py:43
  46.0 2.0 fusion.19
  48.0 98.3 %all-to-all-done = bf16[192,64,64]{0,2,1:T(8,128)(2,1)} async-done(((bf16[192,64,64]{0,2,1:T(8,128)(2,1)}), bf16[192,64,64]{0,2,1:T(8,128)(2,1)}, u32[]{:S(2)}, u32[]{:S(2)}) %all-to-all-start) | async-done | bytes 1572896 | tf_op jit(solution)/shard_map/all_to_all | solution.py:43
  146.3 2.8 copy.30
  149.1 0.0 copy-start.2
  149.1 3.8 %reshape.112 = bf16[12,1024,64]{1,0,2:T(8,128)(2,1)} reshape(bf16[64,192,64]{1,0,2:T(8,128)(2,1)S(1)} %copy.30) | data formatting | bytes 3145728 | tf_op jit(solution)/shard_map/reshape.2
  152.9 0.0 copy-done.2
  152.9 4.4 %fusion.33 = bf16[8,8,12,1024]{3,1,0,2:T(8,128)(2,1)S(1)} fusion(f32[1024]{0:T(1024)S(1)} %bitcast.50, bf16[1024,1024,1]{1,0,2:T(8,128)(2,1)} %bitcast.48, bf16[12,1024,64]{1,0,2:T(8,128)(2,1)} %reshape.112), kind=kOutput, calls=%fused_computation.44 | convolution fusion | flops 1612185600 | bytes 5246976 | tf_op jit(solution)/shard_map/gqp,npgc->nqgc/dot_general | solution.py:52
  157.3 1.3 copy.36
  158.6 3.6 %all_to_all.30 = bf16[64,192,64]{1,0,2:T(8,128)(2,1)S(1)} reshape(bf16[12288,64]{0,1:T(8,128)(2,1)} %bitcast.46) | data formatting | bytes 3145728 | tf_op jit(solution)/shard_map/all_to_all | solution.py:55
  162.2 1.2 copy.34
  163.3 105.3 %all_to_all.37 = bf16[64,192,64]{1,2,0:T(8,128)(2,1)S(1)} all-to-all(bf16[64,192,64]{1,2,0:T(8,128)(2,1)S(1)} %copy.34), channel_id=1, replica_groups=mesh['sp'=64,'dp_0'=4,'dp_1'=2] {'sp'}, dimensions={0} | all-to-all | bytes 3145728 | tf_op jit(solution)/shard_map/all_to_all | solution.py:55
  268.7 2.5 convert_element_type.61
  271.2 3.7 %copy.35 = f32[1,192,4096]{2,1,0:T(8,128)S(1)} copy(f32[1,192,4096]{1,2,0:T(8,128)} %bitcast.45) | data formatting | bytes 6291456 | tf_op jit(solution)/shard_map/convert_element_type | solution.py:57
  274.9 3.7 %fusion.26 = bf16[1,192,4096]{2,1,0:T(8,128)(2,1)} fusion(f32[1,192,4096]{2,1,0:T(8,128)S(1)} %copy.35, bf16[1,192,4096]{2,1,0:T(8,128)(2,1)} %param.6), kind=kLoop, calls=%fused_computation.34 | loop fusion | flops 8650752 | bytes 6291456 | tf_op jit(solution)/shard_map/convert_element_type | solution.py:58
  (3 shorter events, 0.0 us)
Async XLA Ops:
  0.0 6.4 %copy-start = (f32[4096]{0:T(1024)S(1)}, f32[4096]{0:T(1024)}, u32[]{:S(2)}) copy-start(f32[4096]{0:T(1024)} %param.8) | copy-start | bytes 49156
  0.0 6.4 %copy-start.1 = (f32[4096]{0:T(1024)S(1)}, f32[4096]{0:T(1024)}, u32[]{:S(2)}) copy-start(f32[4096]{0:T(1024)} %param.9) | copy-start | bytes 49156
  2.1 19.4 %all-to-all-start.1 = ((bf16[4,1,1,128,1024]{4,3,2,1,0:T(8,128)(2,1)}), bf16[4,1,1,128,1024]{4,3,2,1,0:T(8,128)(2,1)S(1)}, u32[]{:S(2)}, u32[]{:S(2)}) async-start(bf16[4,1,1,128,1024]{4,3,2,1,0:T(8,128)(2,1)} %stack.6), calls=%async_computation.1 | async-start | bytes 2097152 | tf_op jit(solution)/shard_map/all_to_all | solution.py:23
  27.1 119.3 %all-to-all-start = ((bf16[192,64,64]{0,2,1:T(8,128)(2,1)}), bf16[192,64,64]{0,2,1:T(8,128)(2,1)}, u32[]{:S(2)}, u32[]{:S(2)}) async-start(bf16[192,64,64]{0,2,1:T(8,128)(2,1)} %fusion.18), calls=%async_computation | async-start | bytes 4194304 | tf_op jit(solution)/shard_map/all_to_all | solution.py:43
  149.1 3.8 %copy-start.2 = (f32[1,1024]{1,0:T(1,128)S(1)}, f32[1,1024]{1,0:T(1,128)}, u32[]{:S(2)}) copy-start(f32[1,1024]{1,0:T(1,128)} %param.11) | copy-start | bytes 12292
